TPU v7x, 32 devices: a whole 2x2x4 slice. The times are simulated.
32 devices in a mesh: dp: 4 (over y, x), kv: 4 (over z), tp: 2 (over core).
Axes of the slice: x: 2, y: 2, z: 4, core: 2. Of those that a mesh axis runs over, the one named last changes fastest.
Arguments:
- resid: bfloat16 [16, 2048], P('dp', ('kv', 'tp')), may hold values from -45 to 45
- norm_gain: bfloat16 [3, 2048], P(None, ('kv', 'tp')), may hold values from 0.099609375 to 1.8984375
- ffn_gate: bfloat16 [2, 2048, 5632], P(None, None, ('kv', 'tp')), may hold values from -0.125 to 0.125
- ffn_up: bfloat16 [2, 2048, 5632], P(None, None, ('kv', 'tp')), may hold values from -0.125 to 0.125
- ffn_down: bfloat16 [2, 5632, 2048], P(None, ('kv', 'tp')), may hold values from -0.109375 to 0.109375
- w_x: bfloat16 [2048, 64, 64], P(None, 'kv', 'tp'), may hold values from -0.125 to 0.125
- w_z: bfloat16 [2048, 64, 64], P(None, 'kv', 'tp'), may hold values from -0.125 to 0.125
- w_bc: bfloat16 [2048, 2, 8, 128], P('kv'), may hold values from -0.125 to 0.125
- w_dt: bfloat16 [2048, 64], P('kv'), may hold values from -0.125 to 0.125
- dt_bias: float32 [64], replicated, may hold values from -2 to 0.5
- a_log: float32 [64], replicated, may hold values from -1.5 to 1.5
- d_skip: float32 [64], replicated, may hold values from 0.5 to 1.5
- conv_wx: bfloat16 [4, 64, 64], P(None, None, 'tp'), may hold values from -3 to 3
- conv_wbc: bfloat16 [4, 2, 8, 128], replicated, may hold values from -3 to 3
- conv_x: bfloat16 [16, 3, 64, 64], P(('dp', 'kv'), None, None, 'tp'), may hold values from -6 to 6
- conv_bc: bfloat16 [16, 3, 2, 8, 128], P(('dp', 'kv')), may hold values from -6 to 6
- ssm_state: float32 [16, 64, 64, 128], P(('dp', 'kv'), None, 'tp'), may hold values from -3 to 3
- w_out: bfloat16 [64, 64, 2048], P(None, 'tp', 'kv'), may hold values from -0.09375 to 0.09375
Outputs:
- final: bfloat16 [16, 2048], P('dp', ('kv', 'tp'))
All inputs are finite; a program needn't handle non-finite values.
Results may differ from a plain program's by a relative error of at most 0.018.
Values may be sent and summed in bfloat16 or wider, within the bound.
No kernel may reach another device: no remote copies, remote signals or barrier semaphores. Data moves between devices by JAX's collectives and lax.ppermute only.
A program may use at most 64 MiB of HBM per device.

v0:
```python
import jax
import jax.numpy as jnp
from jax import lax
from jax.sharding import PartitionSpec as P

D = 2048
EPS = 1e-06


def normalize(rows, gain):
    values = rows.astype(jnp.float32)
    scale = lax.rsqrt(jnp.mean(values * values, axis=1, keepdims=True) + EPS)
    return (values * scale * gain.astype(jnp.float32).reshape(1, -1)).astype(jnp.bfloat16)


def feed_forward(normed, w_gate, w_up, w_down):
    gate = jnp.dot(normed, w_gate, preferred_element_type=jnp.float32)
    upper = jnp.dot(normed, w_up, preferred_element_type=jnp.float32)
    hidden = (jax.nn.silu(gate) * upper).astype(jnp.bfloat16)
    return jnp.dot(hidden, w_down, preferred_element_type=jnp.float32)


def add_half(base, sums):
    return (base.astype(jnp.float32) + 0.5 * sums).astype(jnp.bfloat16)


def ffn_totals(partial_value):
    return lax.psum(partial_value, ("kv", "tp"))


def short_conv(history, newest, taps):
    window = jnp.concatenate(
        [history.astype(jnp.float32), newest.astype(jnp.float32)[:, None]], axis=1
    )
    return jax.nn.silu(jnp.sum(window * taps.astype(jnp.float32)[None], axis=1))


def state_step(
    xs_new,
    zeta,
    bc_new,
    dt_raw,
    conv_x,
    conv_bc,
    ssm_state,
    conv_wx,
    conv_wbc,
    dt_bias,
    a_log,
    d_skip,
):
    xconv = short_conv(conv_x, xs_new, conv_wx)
    bconv = short_conv(conv_bc, bc_new, conv_wbc)
    heads = xconv.shape[1]
    groups = bconv.shape[2]
    bmat = jnp.repeat(bconv[:, 0], heads // groups, axis=1)
    cmat = jnp.repeat(bconv[:, 1], heads // groups, axis=1)
    step_size = jax.nn.softplus(dt_raw + dt_bias[None, :])
    decay = jnp.exp(-step_size * jnp.exp(a_log)[None, :])
    updated = (
        decay[:, :, None, None] * ssm_state
        + (step_size[:, :, None] * xconv)[..., None] * bmat[:, :, None, :]
    )
    mixed = (
        jnp.einsum("shpn,shn->shp", updated, cmat, precision=lax.Precision.HIGHEST)
        + d_skip[None, :, None] * xconv
    )
    return (mixed * jax.nn.silu(zeta.astype(jnp.float32))).astype(jnp.bfloat16)


def group_terms(slab, w_bc, w_dt):
    span = slab.shape[1]
    flat_bc = w_bc.reshape(span, -1)
    bc_part = jnp.dot(slab, flat_bc, preferred_element_type=jnp.float32)
    dt_part = jnp.dot(slab, w_dt, preferred_element_type=jnp.float32)
    return (
        lax.psum_scatter(bc_part, "kv", scatter_dimension=0, tiled=True),
        lax.psum_scatter(dt_part, "kv", scatter_dimension=0, tiled=True),
    )


def mix_partial(
    normed,
    w_x,
    w_z,
    w_bc,
    w_dt,
    dt_bias,
    a_log,
    d_skip,
    conv_wx,
    conv_wbc,
    conv_x,
    conv_bc,
    ssm_state,
    w_out,
):
    rows = normed.shape[0]
    local_heads = w_x.shape[1]
    half = w_x.shape[2]
    xs_part = (
        jnp.dot(normed, w_x.reshape(D, -1), preferred_element_type=jnp.float32)
        .astype(jnp.bfloat16)
        .reshape(rows, local_heads, half)
    )
    zeta_part = (
        jnp.dot(normed, w_z.reshape(D, -1), preferred_element_type=jnp.float32)
        .astype(jnp.bfloat16)
        .reshape(rows, local_heads, half)
    )
    xs_new, zeta = (
        lax.all_to_all(xs_part, "kv", split_axis=0, concat_axis=1, tiled=True),
        lax.all_to_all(zeta_part, "kv", split_axis=0, concat_axis=1, tiled=True),
    )
    span = w_bc.shape[0]
    slab = lax.dynamic_slice_in_dim(normed, lax.axis_index("kv") * span, span, 1)
    bc_sum, dt_raw = group_terms(slab, w_bc, w_dt)
    bc_new = bc_sum.astype(jnp.bfloat16).reshape((bc_sum.shape[0],) + w_bc.shape[1:])
    mixed = state_step(
        xs_new,
        zeta,
        bc_new,
        dt_raw,
        conv_x,
        conv_bc,
        ssm_state,
        conv_wx,
        conv_wbc,
        dt_bias,
        a_log,
        d_skip,
    )
    flat_out = w_out.reshape(-1, w_out.shape[2])
    piece = lax.all_gather(mixed, "kv", axis=0, tiled=True)
    return jnp.dot(piece.reshape(piece.shape[0], -1), flat_out, preferred_element_type=jnp.float32)


def per_device(
    resid,
    norm_gain,
    ffn_gate,
    ffn_up,
    ffn_down,
    w_x,
    w_z,
    w_bc,
    w_dt,
    dt_bias,
    a_log,
    d_skip,
    conv_wx,
    conv_wbc,
    conv_x,
    conv_bc,
    ssm_state,
    w_out,
):
    mixer_args = (
        w_x,
        w_z,
        w_bc,
        w_dt,
        dt_bias,
        a_log,
        d_skip,
        conv_wx,
        conv_wbc,
        conv_x,
        conv_bc,
        ssm_state,
        w_out,
    )
    rows, gains = (
        lax.all_gather(resid, ("kv", "tp"), axis=1, tiled=True),
        lax.all_gather(norm_gain, ("kv", "tp"), axis=1, tiled=True),
    )
    first = add_half(
        rows,
        ffn_totals(feed_forward(normalize(rows, gains[0]), ffn_gate[0], ffn_up[0], ffn_down[0])),
    )
    partial_value = mix_partial(normalize(first, gains[1]), *mixer_args)
    span = partial_value.shape[1]
    block = lax.dynamic_slice_in_dim(first, lax.axis_index("kv") * span, span, 1)
    joined = (block.astype(jnp.float32) + lax.psum(partial_value, "tp")).astype(jnp.bfloat16)
    second = lax.all_gather(joined, "kv", axis=1, tiled=True)
    final = add_half(
        second,
        ffn_totals(feed_forward(normalize(second, gains[2]), ffn_gate[1], ffn_up[1], ffn_down[1])),
    )
    width = resid.shape[1]
    return lax.dynamic_slice_in_dim(final, lax.axis_index(("kv", "tp")) * width, width, 1)


def solution(mesh):
    placed = (
        P("dp", ("kv", "tp")),
        P(None, ("kv", "tp")),
        P(None, None, ("kv", "tp")),
        P(None, None, ("kv", "tp")),
        P(None, ("kv", "tp"), None),
        P(None, "kv", "tp"),
        P(None, "kv", "tp"),
        P("kv", None, None, None),
        P("kv", None),
        P(),
        P(),
        P(),
        P(None, None, "tp"),
        P(),
        P(("dp", "kv"), None, None, "tp"),
        P(("dp", "kv"), None, None, None, None),
        P(("dp", "kv"), None, "tp", None),
        P(None, "tp", "kv"),
    )
    return jax.shard_map(
        per_device, mesh=mesh, in_specs=placed, out_specs=P("dp", ("kv", "tp")), check_vma=False
    )
```

profile of v0, /device:TPU:0, one launch (start us, length us, event | category | flops | bytes accessed | tf_op | source)
XLA Modules:
  0.0 168.5 jit_solution(16530086735748407296)
XLA Ops:
  0.0 14.7 %all_gather.12 = bf16[4,2048]{1,0:T(4,128)(2,1)S(1)} all-gather(bf16[4,256]{1,0:T(4,128)(2,1)} %param.18), channel_id=1, replica_groups=mesh['dp'=4,'kv'=4,'tp'=2] {'kv','tp'}, dimensions={1}, use_global_device_ids=true | all-gather | bytes 18432 | tf_op jit(solution)/shard_map/all_gather | solution.py:174
  14.9 12.9 %all_gather.13 = bf16[3,2048]{1,0:T(4,128)(2,1)S(1)} all-gather(bf16[3,256]{1,0:T(4,128)(2,1)} %param.19), channel_id=1, replica_groups=mesh['dp'=4,'kv'=4,'tp'=2] {'kv','tp'}, dimensions={1}, use_global_device_ids=true | all-gather | bytes 13824 | tf_op jit(solution)/shard_map/all_gather | solution.py:175
  27.8 2.7 %fusion.10 = f32[4,704]{1,0:T(4,128)S(1)} fusion(bf16[2,2048,704]{1,2,0:T(8,128)(2,1)} %param.20, bf16[4,2048]{1,0:T(4,128)(2,1)S(1)} %all_gather.12, f32[2048]{0:T(1024)S(1)} %bitcast.113, f32[4]{0:T(128)S(1)} %add_rsqrt_fusion.2), kind=kOutput, calls=%fused_computation.10 | convolution fusion | flops 11567104 | bytes 2919440 | tf_op jit(solution)/shard_map/dot_general | solution.py:17
  30.5 4.4 %fusion.6 = f32[4,2048]{1,0:T(4,128)S(1)} fusion(bf16[2,704,2048]{2,1,0:T(8,128)(2,1)} %param.22, bf16[2,2048,704]{1,2,0:T(8,128)(2,1)} %param.21, f32[4,704]{1,0:T(4,128)S(1)} %fusion.10, bf16[4,2048]{1,0:T(4,128)(2,1)S(1)} %all_gather.12, f32[2048]{0:T(1024)S(1)} %bitcast.114, f32[4]{0:T(128)S(1)} %add_rsqrt_fusion.2), kind=kOutput, calls=%fused_computation.6 | convolution fusion | flops 23118336 | bytes 5835792 | tf_op jit(solution)/shard_map/dot_general | solution.py:20
  34.8 26.7 %psum.21 = f32[4,2048]{1,0:T(4,128)S(1)} all-reduce(f32[4,2048]{1,0:T(4,128)S(1)} %fusion.6), channel_id=1, replica_groups=mesh['dp'=4,'kv'=4,'tp'=2] {'kv','tp'}, use_global_device_ids=true, to_apply=%region_1.2 | all-reduce | flops 8192 | bytes 65536 | tf_op jit(solution)/shard_map/psum | solution.py:28
  61.8 0.6 convolution_convert_fusion.1
  62.5 0.7 reshape.219
  63.2 3.2 %all-to-all-start = ((bf16[4,2,256]{2,1,0:T(2,128)(2,1)}), bf16[4,2,256]{2,1,0:T(2,128)(2,1)S(1)}, u32[]{:S(2)}, u32[]{:S(2)}) async-start(bf16[4,2,256]{2,1,0:T(2,128)(2,1)} %reshape.219), calls=%async_computation | async-start | bytes 8192 | tf_op jit(solution)/shard_map/all_to_all | solution.py:112
  66.5 2.2 %convolution_convert_fusion = bf16[4,512]{1,0:T(4,128)(2,1)S(1)} fusion(bf16[4,2048]{1,0:T(4,128)(2,1)S(1)} %fusion.47, bf16[2048,512]{0,1:T(8,128)(2,1)} %bitcast.109), kind=kOutput, calls=%fused_computation.26 | convolution fusion | flops 8390656 | bytes 2117632 | tf_op jit(solution)/shard_map/dot_general | solution.py:107
  68.9 2.0 %fusion.18 = f32[4,2048]{1,0:T(4,128)S(1)} fusion(bf16[64,8,16,128]{3,2,1,0:T(8,128)(2,1)} %bitcast.108, bf16[4,2048]{1,0:T(4,128)(2,1)S(1)} %fusion.47, s32[]{:T(128)S(6)} %select_n.11), kind=kOutput, calls=%fused_computation.18 | convolution fusion | flops 8388608 | bytes 2134020 | tf_op jit(solution)/shard_map/dot_general | solution.py:74
  71.4 19.8 %all-reduce.2 = (bf16[4,2048]{1,0:T(4,128)(2,1)S(1)}, f32[4,64]{1,0:T(4,128)S(1)}) all-reduce(f32[4,2048]{1,0:T(4,128)S(1)} %fusion.18, f32[4,64]{1,0:T(4,128)S(1)} %fusion.69), channel_id=4, replica_groups=mesh['dp'=4,'kv'=4,'tp'=2] {'kv'}, use_global_device_ids=true, to_apply=%region_5.6.clone | all-reduce | flops 8448 | bytes 51200
  91.2 0.7 fusion.60
  92.1 0.7 reshape.217
  92.8 3.2 %all-to-all-start.1 = ((bf16[4,2,256]{2,1,0:T(2,128)(2,1)}), bf16[4,2,256]{2,1,0:T(2,128)(2,1)S(1)}, u32[]{:S(2)}, u32[]{:S(2)}) async-start(bf16[4,2,256]{2,1,0:T(2,128)(2,1)} %reshape.217), calls=%async_computation.1 | async-start | bytes 8192 | tf_op jit(solution)/shard_map/all_to_all | solution.py:113
  96.0 0.7 fusion.75
  96.9 4.7 %all-to-all-done.1 = bf16[4,2,256]{2,1,0:T(2,128)(2,1)S(1)} async-done(((bf16[4,2,256]{2,1,0:T(2,128)(2,1)}), bf16[4,2,256]{2,1,0:T(2,128)(2,1)S(1)}, u32[]{:S(2)}, u32[]{:S(2)}) %all-to-all-start.1) | async-done | bytes 4128 | tf_op jit(solution)/shard_map/all_to_all | solution.py:113
  101.9 1.9 %fusion.33 = f32[64,1,32]{2,1,0:T(1,128)S(1)} fusion(f32[64,128,1]{1,2,0:T(1,128)S(1)} %bitcast.110, f32[1,64,32,128]{3,2,1,0:T(8,128)S(1)} %copy-done.1, f32[64,128]{1,0:T(8,128)S(1)} %broadcast_bitcast_fusion, f32[64,32]{1,0:T(8,128)S(1)} %copy.28, f32[64]{0:T(128)S(1)} %get-tuple-element.7), kind=kOutput, calls=%fused_computation.28 | convolution fusion | flops 3932160 | bytes 1130752 | tf_op jit(solution)/shard_map/shpn,shn->shp/dot_general | solution.py:65
  103.9 13.1 %all-gather.1 = bf16[4,64,32]{1,2,0:T(8,128)(2,1)S(1)} all-gather(bf16[1,64,32]{1,2,0:T(8,128)(2,1)S(1)} %fusion.64), channel_id=2, replica_groups=mesh['dp'=4,'kv'=4,'tp'=2] {'kv'}, dimensions={0}, use_global_device_ids=true | all-gather | bytes 20480 | tf_op jit(solution)/shard_map/all_gather | solution.py:134
  117.1 2.0 %convolution_bitcast_fusion = f32[4,512]{1,0:T(4,128)S(1)} fusion(bf16[4,64,32]{2,0,1:T(4,128)(2,1)S(1)} %copy.35, bf16[64,32,512]{2,1,0:T(8,128)(2,1)} %param.35), kind=kOutput, calls=%fused_computation.25 | convolution fusion | flops 8388608 | bytes 2121728 | tf_op jit(solution)/shard_map/dot_general | solution.py:135
  119.2 2.5 %psum.22 = f32[4,512]{1,0:T(4,128)S(1)} all-reduce(f32[4,512]{1,0:T(4,128)S(1)} %convolution_bitcast_fusion), channel_id=1, replica_groups=mesh['dp'=4,'kv'=4,'tp'=2] {'tp'}, use_global_device_ids=true, to_apply=%region_7.8 | all-reduce | flops 2048 | bytes 16384 | tf_op jit(solution)/shard_map/psum | solution.py:184
  121.6 13.2 %all_gather.15 = bf16[4,2048]{1,0:T(4,128)(2,1)S(1)} all-gather(bf16[4,512]{1,0:T(4,128)(2,1)S(1)} %add_convert_fusion), channel_id=1, replica_groups=mesh['dp'=4,'kv'=4,'tp'=2] {'kv'}, dimensions={1}, use_global_device_ids=true | all-gather | bytes 20480 | tf_op jit(solution)/shard_map/all_gather | solution.py:185
  135.0 2.7 %fusion.4 = f32[4,704]{1,0:T(4,128)S(1)} fusion(bf16[2,2048,704]{1,2,0:T(8,128)(2,1)} %param.20, f32[2048]{0:T(1024)S(1)} %bitcast.111, f32[4]{0:T(128)S(1)} %add_rsqrt_fusion, bf16[4,2048]{1,0:T(4,128)(2,1)S(1)} %all_gather.15), kind=kOutput, calls=%fused_computation.4 | convolution fusion | flops 11567104 | bytes 2919440 | tf_op jit(solution)/shard_map/dot_general | solution.py:17
  137.7 4.4 %fusion = f32[4,2048]{1,0:T(4,128)S(1)} fusion(bf16[2,704,2048]{2,1,0:T(8,128)(2,1)} %param.22, bf16[2,2048,704]{1,2,0:T(8,128)(2,1)} %param.21, f32[4,704]{1,0:T(4,128)S(1)} %fusion.4, f32[2048]{0:T(1024)S(1)} %bitcast.112, f32[4]{0:T(128)S(1)} %add_rsqrt_fusion, bf16[4,2048]{1,0:T(4,128)(2,1)S(1)} %all_gather.15), kind=kOutput, calls=%fused_computation | convolution fusion | flops 23118336 | bytes 5835792 | tf_op jit(solution)/shard_map/dot_general | solution.py:20
  142.0 25.9 %psum.23 = f32[4,2048]{1,0:T(4,128)S(1)} all-reduce(f32[4,2048]{1,0:T(4,128)S(1)} %fusion), channel_id=1, replica_groups=mesh['dp'=4,'kv'=4,'tp'=2] {'kv','tp'}, use_global_device_ids=true, to_apply=%region_9.10 | all-reduce | flops 8192 | bytes 65536 | tf_op jit(solution)/shard_map/psum | solution.py:28
  (54 shorter events, 2.8 us)
Async XLA Ops:
  0.0 61.7 %copy-start = (bf16[2048,16,32]{0,2,1:T(8,128)(2,1)S(1)}, bf16[2048,16,32]{0,2,1:T(8,128)(2,1)}, u32[]{:S(2)}) copy-start(bf16[2048,16,32]{0,2,1:T(8,128)(2,1)} %param.23) | copy-start | bytes 6291460
  34.8 33.9 %copy-start.2 = (bf16[512,64]{0,1:T(8,128)(2,1)S(1)}, bf16[512,64]{0,1:T(8,128)(2,1)}, u32[]{:S(2)}) copy-start(bf16[512,64]{0,1:T(8,128)(2,1)} %param.26) | copy-start | bytes 196612
  61.7 9.1 %copy-start.10 = (u32[32]{0:T(128)S(1)}, u32[32]{0:T(128)}, u32[]{:S(2)}) copy-start(u32[32]{0:T(128)} %constant.45) | copy-start | bytes 388
  61.7 30.2 %copy-start.5 = (bf16[4,2,8,128]{3,2,1,0:T(8,128)(2,1)S(1)}, bf16[4,2,8,128]{3,2,1,0:T(8,128)(2,1)}, u32[]{:S(2)}) copy-start(bf16[4,2,8,128]{3,2,1,0:T(8,128)(2,1)} %param.31) | copy-start | bytes 49156
  61.8 30.2 %copy-start.6 = (bf16[1,3,2,8,128]{4,3,2,1,0:T(8,128)(2,1)S(1)}, bf16[1,3,2,8,128]{4,3,2,1,0:T(8,128)(2,1)}, u32[]{:S(2)}) copy-start(bf16[1,3,2,8,128]{4,3,2,1,0:T(8,128)(2,1)} %param.33) | copy-start | bytes 36868
  61.8 34.2 %copy-start.8 = (f32[64]{0:T(128)S(1)}, f32[64]{0:T(128)}, u32[]{:S(2)}) copy-start(f32[64]{0:T(128)} %param.28) | copy-start | bytes 772
  61.8 34.2 %copy-start.9 = (f32[64]{0:T(128)S(1)}, f32[64]{0:T(128)}, u32[]{:S(2)}) copy-start(f32[64]{0:T(128)} %param.27) | copy-start | bytes 772
  62.4 39.3 %copy-start.3 = (bf16[4,64,32]{1,2,0:T(8,128)(2,1)S(1)}, bf16[4,64,32]{1,2,0:T(8,128)(2,1)}, u32[]{:S(2)}) copy-start(bf16[4,64,32]{1,2,0:T(8,128)(2,1)} %param.30) | copy-start | bytes 49156
  62.4 39.3 %copy-start.4 = (bf16[1,3,64,32]{2,3,1,0:T(8,128)(2,1)S(1)}, bf16[1,3,64,32]{2,3,1,0:T(8,128)(2,1)}, u32[]{:S(2)}) copy-start(bf16[1,3,64,32]{2,3,1,0:T(8,128)(2,1)} %param.32) | copy-start | bytes 36868
  62.4 39.4 %copy-start.1 = (f32[1,64,32,128]{3,2,1,0:T(8,128)S(1)}, f32[1,64,32,128]{3,2,1,0:T(8,128)}, u32[]{:S(2)}) copy-start(f32[1,64,32,128]{3,2,1,0:T(8,128)} %param.34) | copy-start | bytes 3145732
  63.2 29.5 %all-to-all-start = ((bf16[4,2,256]{2,1,0:T(2,128)(2,1)}), bf16[4,2,256]{2,1,0:T(2,128)(2,1)S(1)}, u32[]{:S(2)}, u32[]{:S(2)}) async-start(bf16[4,2,256]{2,1,0:T(2,128)(2,1)} %reshape.219), calls=%async_computation | async-start | bytes 8192 | tf_op jit(solution)/shard_map/all_to_all | solution.py:112
  66.5 37.4 %copy-start.7 = (f32[64]{0:T(128)S(1)}, f32[64]{0:T(128)}, u32[]{:S(2)}) copy-start(f32[64]{0:T(128)} %param.29) | copy-start | bytes 772
  92.8 8.8 %all-to-all-start.1 = ((bf16[4,2,256]{2,1,0:T(2,128)(2,1)}), bf16[4,2,256]{2,1,0:T(2,128)(2,1)S(1)}, u32[]{:S(2)}, u32[]{:S(2)}) async-start(bf16[4,2,256]{2,1,0:T(2,128)(2,1)} %reshape.217), calls=%async_computation.1 | async-start | bytes 8192 | tf_op jit(solution)/shard_map/all_to_all | solution.py:113
where the time goes:
time: 169 us
  blocking collectives  129 us (76%)
  matrix products  22.9 us (14%)
  starting transfers between devices  6.47 us (4%)
  waiting for transfers between devices  4.68 us (3%)
  local copies, waits for them, and re-layouts  3.47 us (2%)
  other arithmetic  1.89 us (1%)
    psum x2, blocking collectives, ffn_totals(): return lax.psum(partial_value, ('kv', 'tp'))  52.6 us
    unnamed x1, blocking collectives  19.8 us
    all_gather x1, blocking collectives, per_device(): lax.all_gather(resid, ('kv', 'tp'), axis=1, tiled=True)  14.7 us
    all_gather x1, blocking collectives, per_device(): second = lax.all_gather(joined, 'kv', axis=1, tiled=True)  13.2 us
    all_gather x1, blocking collectives, mix_partial(): piece = lax.all_gather(mixed, 'kv', axis=0, tiled=True)  13.1 us
    all_gather x1, blocking collectives, per_device(): lax.all_gather(norm_gain, ('kv', 'tp'), axis=1, tiled=True)  12.9 us
    dot_general x2, matrix products, feed_forward(): return jnp.dot(hidden, w_down, preferred_element_type=jnp.float32)  8.72 us
    dot_general x2, matrix products, feed_forward(): gate = jnp.dot(normed, w_gate, preferred_element_type=jnp.float32)  5.31 us
  transfers between devices with their start and end apart: 2, of which 1 were waited for; matrix products, arithmetic and copies ran while one was open for 4% of the time, Pallas kernels for 0%

commit v1 on v0

--- a/solution.py
+++ b/solution.py
@@ -25,7 +25,7 @@
 
 
 def ffn_totals(partial_value):
-    return lax.psum(partial_value, ("kv", "tp"))
+    return lax.psum(lax.psum(partial_value, "kv"), "tp")
 
 
 def short_conv(history, newest, taps):

time: 169 us -> 156 us (0.923)
  blocking collectives: 129 us -> 116 us
    psum x2 -> x4, blocking collectives: 52.6 us -> 39.6 us  [ffn_totals(): return lax.psum(lax.psum(partial_value, 'kv'), 'tp')]
  transfers between devices with their start and end apart: 2 -> 2, of which waited for: 1 -> 1; matrix products, arithmetic and copies ran while one was open for 4% -> 5% of each run, Pallas kernels for 0% -> 0%
where the time goes in v1:
time: 156 us
  blocking collectives  116 us (74%)
  matrix products  22.9 us (15%)
  starting transfers between devices  6.47 us (4%)
  waiting for transfers between devices  4.68 us (3%)
  local copies, waits for them, and re-layouts  3.47 us (2%)
  other arithmetic  1.9 us (1%)
    psum x4, blocking collectives, ffn_totals(): return lax.psum(lax.psum(partial_value, 'kv'), 'tp')  39.6 us
    unnamed x1, blocking collectives  19.8 us
    all_gather x1, blocking collectives, per_device(): lax.all_gather(resid, ('kv', 'tp'), axis=1, tiled=True)  14.7 us
    all_gather x1, blocking collectives, per_device(): second = lax.all_gather(joined, 'kv', axis=1, tiled=True)  13.2 us
    all_gather x1, blocking collectives, mix_partial(): piece = lax.all_gather(mixed, 'kv', axis=0, tiled=True)  13.1 us
    all_gather x1, blocking collectives, per_device(): lax.all_gather(norm_gain, ('kv', 'tp'), axis=1, tiled=True)  12.9 us
    dot_general x2, matrix products, feed_forward(): return jnp.dot(hidden, w_down, preferred_element_type=jnp.float32)  8.72 us
    dot_general x2, matrix products, feed_forward(): gate = jnp.dot(normed, w_gate, preferred_element_type=jnp.float32)  5.31 us
  transfers between devices with their start and end apart: 2, of which 1 were waited for; matrix products, arithmetic and copies ran while one was open for 5% of the time, Pallas kernels for 0%

profile of v1, /device:TPU:0, one launch (start us, length us, event | category | flops | bytes accessed | tf_op | source)
XLA Modules:
  0.0 155.6 jit_solution(6570567856445073053)
XLA Ops:
  0.0 14.7 %all_gather.12 = bf16[4,2048]{1,0:T(4,128)(2,1)S(1)} all-gather(bf16[4,256]{1,0:T(4,128)(2,1)} %param.18), channel_id=1, replica_groups=mesh['dp'=4,'kv'=4,'tp'=2] {'kv','tp'}, dimensions={1}, use_global_device_ids=true | all-gather | bytes 18432 | tf_op jit(solution)/shard_map/all_gather | solution.py:174
  14.9 12.9 %all_gather.13 = bf16[3,2048]{1,0:T(4,128)(2,1)S(1)} all-gather(bf16[3,256]{1,0:T(4,128)(2,1)} %param.19), channel_id=1, replica_groups=mesh['dp'=4,'kv'=4,'tp'=2] {'kv','tp'}, dimensions={1}, use_global_device_ids=true | all-gather | bytes 13824 | tf_op jit(solution)/shard_map/all_gather | solution.py:175
  27.8 2.7 %fusion.10 = f32[4,704]{1,0:T(4,128)S(1)} fusion(bf16[2,2048,704]{1,2,0:T(8,128)(2,1)} %param.20, bf16[4,2048]{1,0:T(4,128)(2,1)S(1)} %all_gather.12, f32[2048]{0:T(1024)S(1)} %bitcast.113, f32[4]{0:T(128)S(1)} %add_rsqrt_fusion.2), kind=kOutput, calls=%fused_computation.10 | convolution fusion | flops 11567104 | bytes 2919440 | tf_op jit(solution)/shard_map/dot_general | solution.py:17
  30.5 4.4 %fusion.6 = f32[4,2048]{1,0:T(4,128)S(1)} fusion(bf16[2,704,2048]{2,1,0:T(8,128)(2,1)} %param.22, bf16[2,2048,704]{1,2,0:T(8,128)(2,1)} %param.21, f32[4,704]{1,0:T(4,128)S(1)} %fusion.10, bf16[4,2048]{1,0:T(4,128)(2,1)S(1)} %all_gather.12, f32[2048]{0:T(1024)S(1)} %bitcast.114, f32[4]{0:T(128)S(1)} %add_rsqrt_fusion.2), kind=kOutput, calls=%fused_computation.6 | convolution fusion | flops 23118336 | bytes 5835792 | tf_op jit(solution)/shard_map/dot_general | solution.py:20
  34.8 16.6 %psum.35 = f32[4,2048]{1,0:T(4,128)S(1)} all-reduce(f32[4,2048]{1,0:T(4,128)S(1)} %fusion.6), channel_id=1, replica_groups=mesh['dp'=4,'kv'=4,'tp'=2] {'kv'}, use_global_device_ids=true, to_apply=%region_1.2 | all-reduce | flops 8192 | bytes 65536 | tf_op jit(solution)/shard_map/psum | solution.py:28
  51.4 3.4 %psum.36 = f32[4,2048]{1,0:T(4,128)S(1)} all-reduce(f32[4,2048]{1,0:T(4,128)S(1)} %psum.35), channel_id=1, replica_groups=mesh['dp'=4,'kv'=4,'tp'=2] {'tp'}, use_global_device_ids=true, to_apply=%region_2.3 | all-reduce | flops 8192 | bytes 65536 | tf_op jit(solution)/shard_map/psum | solution.py:28
  55.9 0.7 reshape.219
  56.6 3.2 %all-to-all-start = ((bf16[4,2,256]{2,1,0:T(2,128)(2,1)}), bf16[4,2,256]{2,1,0:T(2,128)(2,1)S(1)}, u32[]{:S(2)}, u32[]{:S(2)}) async-start(bf16[4,2,256]{2,1,0:T(2,128)(2,1)} %reshape.219), calls=%async_computation | async-start | bytes 8192 | tf_op jit(solution)/shard_map/all_to_all | solution.py:112
  59.8 2.2 %convolution_convert_fusion = bf16[4,512]{1,0:T(4,128)(2,1)S(1)} fusion(bf16[4,2048]{1,0:T(4,128)(2,1)S(1)} %fusion.47, bf16[2048,512]{0,1:T(8,128)(2,1)} %bitcast.109), kind=kOutput, calls=%fused_computation.26 | convolution fusion | flops 8390656 | bytes 2117632 | tf_op jit(solution)/shard_map/dot_general | solution.py:107
  62.2 2.0 %fusion.18 = f32[4,2048]{1,0:T(4,128)S(1)} fusion(bf16[64,8,16,128]{3,2,1,0:T(8,128)(2,1)} %bitcast.108, bf16[4,2048]{1,0:T(4,128)(2,1)S(1)} %fusion.47, s32[]{:T(128)S(6)} %select_n.11), kind=kOutput, calls=%fused_computation.18 | convolution fusion | flops 8388608 | bytes 2134020 | tf_op jit(solution)/shard_map/dot_general | solution.py:74
  64.8 19.8 %all-reduce.2 = (bf16[4,2048]{1,0:T(4,128)(2,1)S(1)}, f32[4,64]{1,0:T(4,128)S(1)}) all-reduce(f32[4,2048]{1,0:T(4,128)S(1)} %fusion.18, f32[4,64]{1,0:T(4,128)S(1)} %fusion.69), channel_id=4, replica_groups=mesh['dp'=4,'kv'=4,'tp'=2] {'kv'}, use_global_device_ids=true, to_apply=%region_6.7.clone | all-reduce | flops 8448 | bytes 51200
  84.6 0.7 fusion.60
  85.4 0.7 reshape.217
  86.1 3.2 %all-to-all-start.1 = ((bf16[4,2,256]{2,1,0:T(2,128)(2,1)}), bf16[4,2,256]{2,1,0:T(2,128)(2,1)S(1)}, u32[]{:S(2)}, u32[]{:S(2)}) async-start(bf16[4,2,256]{2,1,0:T(2,128)(2,1)} %reshape.217), calls=%async_computation.1 | async-start | bytes 8192 | tf_op jit(solution)/shard_map/all_to_all | solution.py:113
  90.2 4.7 %all-to-all-done.1 = bf16[4,2,256]{2,1,0:T(2,128)(2,1)S(1)} async-done(((bf16[4,2,256]{2,1,0:T(2,128)(2,1)}), bf16[4,2,256]{2,1,0:T(2,128)(2,1)S(1)}, u32[]{:S(2)}, u32[]{:S(2)}) %all-to-all-start.1) | async-done | bytes 4128 | tf_op jit(solution)/shard_map/all_to_all | solution.py:113
  95.2 1.9 %fusion.33 = f32[64,1,32]{2,1,0:T(1,128)S(1)} fusion(f32[64,128,1]{1,2,0:T(1,128)S(1)} %bitcast.110, f32[1,64,32,128]{3,2,1,0:T(8,128)S(1)} %copy-done.1, f32[64,128]{1,0:T(8,128)S(1)} %broadcast_bitcast_fusion, f32[64,32]{1,0:T(8,128)S(1)} %copy.28, f32[64]{0:T(128)S(1)} %get-tuple-element.7), kind=kOutput, calls=%fused_computation.28 | convolution fusion | flops 3932160 | bytes 1130752 | tf_op jit(solution)/shard_map/shpn,shn->shp/dot_general | solution.py:65
  97.2 13.1 %all-gather.1 = bf16[4,64,32]{1,2,0:T(8,128)(2,1)S(1)} all-gather(bf16[1,64,32]{1,2,0:T(8,128)(2,1)S(1)} %fusion.64), channel_id=2, replica_groups=mesh['dp'=4,'kv'=4,'tp'=2] {'kv'}, dimensions={0}, use_global_device_ids=true | all-gather | bytes 20480 | tf_op jit(solution)/shard_map/all_gather | solution.py:134
  110.5 2.0 %convolution_bitcast_fusion = f32[4,512]{1,0:T(4,128)S(1)} fusion(bf16[4,64,32]{2,0,1:T(4,128)(2,1)S(1)} %copy.35, bf16[64,32,512]{2,1,0:T(8,128)(2,1)} %param.35), kind=kOutput, calls=%fused_computation.25 | convolution fusion | flops 8388608 | bytes 2121728 | tf_op jit(solution)/shard_map/dot_general | solution.py:135
  112.5 2.5 %psum.37 = f32[4,512]{1,0:T(4,128)S(1)} all-reduce(f32[4,512]{1,0:T(4,128)S(1)} %convolution_bitcast_fusion), channel_id=1, replica_groups=mesh['dp'=4,'kv'=4,'tp'=2] {'tp'}, use_global_device_ids=true, to_apply=%region_8.9 | all-reduce | flops 2048 | bytes 16384 | tf_op jit(solution)/shard_map/psum | solution.py:184
  115.0 13.2 %all_gather.15 = bf16[4,2048]{1,0:T(4,128)(2,1)S(1)} all-gather(bf16[4,512]{1,0:T(4,128)(2,1)S(1)} %add_convert_fusion), channel_id=1, replica_groups=mesh['dp'=4,'kv'=4,'tp'=2] {'kv'}, dimensions={1}, use_global_device_ids=true | all-gather | bytes 20480 | tf_op jit(solution)/shard_map/all_gather | solution.py:185
  128.3 2.7 %fusion.4 = f32[4,704]{1,0:T(4,128)S(1)} fusion(bf16[2,2048,704]{1,2,0:T(8,128)(2,1)} %param.20, f32[2048]{0:T(1024)S(1)} %bitcast.111, f32[4]{0:T(128)S(1)} %add_rsqrt_fusion, bf16[4,2048]{1,0:T(4,128)(2,1)S(1)} %all_gather.15), kind=kOutput, calls=%fused_computation.4 | convolution fusion | flops 11567104 | bytes 2919440 | tf_op jit(solution)/shard_map/dot_general | solution.py:17
  131.0 4.4 %fusion = f32[4,2048]{1,0:T(4,128)S(1)} fusion(bf16[2,704,2048]{2,1,0:T(8,128)(2,1)} %param.22, bf16[2,2048,704]{1,2,0:T(8,128)(2,1)} %param.21, f32[4,704]{1,0:T(4,128)S(1)} %fusion.4, f32[2048]{0:T(1024)S(1)} %bitcast.112, f32[4]{0:T(128)S(1)} %add_rsqrt_fusion, bf16[4,2048]{1,0:T(4,128)(2,1)S(1)} %all_gather.15), kind=kOutput, calls=%fused_computation | convolution fusion | flops 23118336 | bytes 5835792 | tf_op jit(solution)/shard_map/dot_general | solution.py:20
  135.4 16.2 %psum.38 = f32[4,2048]{1,0:T(4,128)S(1)} all-reduce(f32[4,2048]{1,0:T(4,128)S(1)} %fusion), channel_id=1, replica_groups=mesh['dp'=4,'kv'=4,'tp'=2] {'kv'}, use_global_device_ids=true, to_apply=%region_10.11 | all-reduce | flops 8192 | bytes 65536 | tf_op jit(solution)/shard_map/psum | solution.py:28
  151.6 3.4 %psum.39 = f32[4,2048]{1,0:T(4,128)S(1)} all-reduce(f32[4,2048]{1,0:T(4,128)S(1)} %psum.38), channel_id=1, replica_groups=mesh['dp'=4,'kv'=4,'tp'=2] {'tp'}, use_global_device_ids=true, to_apply=%region_11.12 | all-reduce | flops 8192 | bytes 65536 | tf_op jit(solution)/shard_map/psum | solution.py:28
  (56 shorter events, 4.1 us)
Async XLA Ops:
  0.0 55.1 %copy-start = (bf16[2048,16,32]{0,2,1:T(8,128)(2,1)S(1)}, bf16[2048,16,32]{0,2,1:T(8,128)(2,1)}, u32[]{:S(2)}) copy-start(bf16[2048,16,32]{0,2,1:T(8,128)(2,1)} %param.23) | copy-start | bytes 6291460
  34.8 27.2 %copy-start.2 = (bf16[512,64]{0,1:T(8,128)(2,1)S(1)}, bf16[512,64]{0,1:T(8,128)(2,1)}, u32[]{:S(2)}) copy-start(bf16[512,64]{0,1:T(8,128)(2,1)} %param.26) | copy-start | bytes 196612
  55.1 9.1 %copy-start.10 = (u32[32]{0:T(128)S(1)}, u32[32]{0:T(128)}, u32[]{:S(2)}) copy-start(u32[32]{0:T(128)} %constant.45) | copy-start | bytes 388
  55.1 30.2 %copy-start.5 = (bf16[4,2,8,128]{3,2,1,0:T(8,128)(2,1)S(1)}, bf16[4,2,8,128]{3,2,1,0:T(8,128)(2,1)}, u32[]{:S(2)}) copy-start(bf16[4,2,8,128]{3,2,1,0:T(8,128)(2,1)} %param.31) | copy-start | bytes 49156
  55.1 30.2 %copy-start.6 = (bf16[1,3,2,8,128]{4,3,2,1,0:T(8,128)(2,1)S(1)}, bf16[1,3,2,8,128]{4,3,2,1,0:T(8,128)(2,1)}, u32[]{:S(2)}) copy-start(bf16[1,3,2,8,128]{4,3,2,1,0:T(8,128)(2,1)} %param.33) | copy-start | bytes 36868
  55.1 34.2 %copy-start.8 = (f32[64]{0:T(128)S(1)}, f32[64]{0:T(128)}, u32[]{:S(2)}) copy-start(f32[64]{0:T(128)} %param.28) | copy-start | bytes 772
  55.1 34.2 %copy-start.9 = (f32[64]{0:T(128)S(1)}, f32[64]{0:T(128)}, u32[]{:S(2)}) copy-start(f32[64]{0:T(128)} %param.27) | copy-start | bytes 772
  55.8 39.3 %copy-start.3 = (bf16[4,64,32]{1,2,0:T(8,128)(2,1)S(1)}, bf16[4,64,32]{1,2,0:T(8,128)(2,1)}, u32[]{:S(2)}) copy-start(bf16[4,64,32]{1,2,0:T(8,128)(2,1)} %param.30) | copy-start | bytes 49156
  55.8 39.3 %copy-start.4 = (bf16[1,3,64,32]{2,3,1,0:T(8,128)(2,1)S(1)}, bf16[1,3,64,32]{2,3,1,0:T(8,128)(2,1)}, u32[]{:S(2)}) copy-start(bf16[1,3,64,32]{2,3,1,0:T(8,128)(2,1)} %param.32) | copy-start | bytes 36868
  55.8 39.4 %copy-start.1 = (f32[1,64,32,128]{3,2,1,0:T(8,128)S(1)}, f32[1,64,32,128]{3,2,1,0:T(8,128)}, u32[]{:S(2)}) copy-start(f32[1,64,32,128]{3,2,1,0:T(8,128)} %param.34) | copy-start | bytes 3145732
  56.6 29.5 %all-to-all-start = ((bf16[4,2,256]{2,1,0:T(2,128)(2,1)}), bf16[4,2,256]{2,1,0:T(2,128)(2,1)S(1)}, u32[]{:S(2)}, u32[]{:S(2)}) async-start(bf16[4,2,256]{2,1,0:T(2,128)(2,1)} %reshape.219), calls=%async_computation | async-start | bytes 8192 | tf_op jit(solution)/shard_map/all_to_all | solution.py:112
  59.8 37.4 %copy-start.7 = (f32[64]{0:T(128)S(1)}, f32[64]{0:T(128)}, u32[]{:S(2)}) copy-start(f32[64]{0:T(128)} %param.29) | copy-start | bytes 772
  86.1 8.8 %all-to-all-start.1 = ((bf16[4,2,256]{2,1,0:T(2,128)(2,1)}), bf16[4,2,256]{2,1,0:T(2,128)(2,1)S(1)}, u32[]{:S(2)}, u32[]{:S(2)}) async-start(bf16[4,2,256]{2,1,0:T(2,128)(2,1)} %reshape.217), calls=%async_computation.1 | async-start | bytes 8192 | tf_op jit(solution)/shard_map/all_to_all | solution.py:113
